TPU v7x, 32 devices: a whole 2x2x4 slice. The times are simulated.
32 devices in a mesh: sp: 8 (over z, y), tp: 4 (over x, core).
Axes of the slice: x: 2, y: 2, z: 4, core: 2. Of those that a mesh axis runs over, the one named last changes fastest.
Arguments:
- tokens: bfloat16 [2560, 2048], P('sp', 'tp'), may hold values from -6 to 6
- pre_gain: float32 [2, 2048], replicated, may hold values from 0.1 to 1.9
- w_value: bfloat16 [2, 2048, 2048], P(None, 'sp', 'tp'), may hold values from -0.125 to 0.125
- w_gate: bfloat16 [2, 2048, 2048], P(None, 'sp', 'tp'), may hold values from -0.125 to 0.125
- taps: float32 [2, 31, 2048], P(None, None, 'tp'), may hold values from -5 to 5
- norm_gain: float32 [2, 2048], P(None, 'tp'), may hold values from 0.1 to 1.9
- norm_shift: float32 [2, 2048], P(None, 'tp'), may hold values from -3 to 3
- w_out: bfloat16 [2, 2048, 2048], P(None, 'tp', 'sp'), may hold values from -2 to 2
- post_gain: float32 [2, 2048], P(None, 'tp'), may hold values from 0.1 to 1.9
Outputs:
- stream: bfloat16 [2560, 2048], P('sp', 'tp')
All inputs are finite; a program needn't handle non-finite values.
Results may differ from a plain program's by a relative error of at most 0.015.
Values may be sent and summed in bfloat16 or wider, within the bound.
A program may use at most 64 MiB of HBM per device.

v0:
```python
import jax
import jax.numpy as jnp
from jax import lax
from jax.sharding import PartitionSpec as P

D = 2048
CONV_WIDTH = 31
LAYERS = 2
EPSILON = 1e-06
LN_EPSILON = 1e-05


def passed_along(block, axis, distance):
    devices = range(lax.axis_size(axis))
    route = [(i - distance, i) for i in devices if i - distance in devices]
    return lax.ppermute(block, axis, route)


def local(tokens, pre_gain, w_value, w_gate, taps, norm_gain, norm_shift, w_out, post_gain):
    stream = tokens
    full_value, full_gate = (
        lax.all_gather(w_value, "sp", axis=1, tiled=True),
        lax.all_gather(w_gate, "sp", axis=1, tiled=True),
    )
    full_out = lax.all_gather(w_out, "sp", axis=2, tiled=True)
    for layer in range(LAYERS):
        whole = lax.all_gather(stream, "tp", axis=1, tiled=True)
        whole_f = whole.astype(jnp.float32)
        normed = (
            whole_f
            * lax.rsqrt(jnp.mean(whole_f * whole_f, -1, keepdims=True) + EPSILON)
            * pre_gain[layer]
        ).astype(jnp.bfloat16)
        value_mat = full_value[layer]
        gate_mat = full_gate[layer]
        out_mat = full_out[layer]
        value_proj = jnp.dot(normed, value_mat, preferred_element_type=jnp.float32)
        gate_proj = jnp.dot(normed, gate_mat, preferred_element_type=jnp.float32)
        glu_act = (value_proj * jax.nn.sigmoid(gate_proj)).astype(jnp.bfloat16)
        rows = glu_act.shape[0]
        fringe = passed_along(glu_act[rows - (CONV_WIDTH - 1) :], "sp", 1)
        padded = jnp.concatenate([fringe, glu_act], 0).astype(jnp.float32)
        conv_out = jnp.zeros(glu_act.shape, jnp.float32)
        for offset in range(CONV_WIDTH):
            conv_out = conv_out + taps[layer, offset] * padded[offset : offset + rows]
        row_sum, row_square = lax.psum(
            (jnp.sum(conv_out, -1, keepdims=True), jnp.sum(conv_out * conv_out, -1, keepdims=True)),
            "tp",
        )
        center = row_sum / D
        spread = jnp.maximum(row_square / D - center * center, 0.0)
        activated = jax.nn.silu(
            (conv_out - center) * lax.rsqrt(spread + LN_EPSILON) * norm_gain[layer]
            + norm_shift[layer]
        ).astype(jnp.bfloat16)
        terms = jnp.dot(activated, out_mat, preferred_element_type=jnp.float32)
        summed = lax.psum_scatter(terms.astype(jnp.bfloat16), "tp", scatter_dimension=1, tiled=True)
        projected = summed.astype(jnp.float32)
        out_square = lax.psum(jnp.sum(projected * projected, -1, keepdims=True), "tp")
        scale = lax.rsqrt(out_square / D + EPSILON)
        stream = (stream.astype(jnp.float32) + projected * scale * post_gain[layer]).astype(
            jnp.bfloat16
        )
    return stream


def solution(mesh):
    placed = (
        P("sp", "tp"),
        P(),
        P(None, "sp", "tp"),
        P(None, "sp", "tp"),
        P(None, None, "tp"),
        P(None, "tp"),
        P(None, "tp"),
        P(None, "tp", "sp"),
        P(None, "tp"),
    )
    return jax.shard_map(
        local, mesh=mesh, in_specs=placed, out_specs=P("sp", "tp"), check_vma=False
    )
```

profile of v0, /device:TPU:0, one launch (start us, length us, event | category | flops | bytes accessed | tf_op | source)
XLA Modules:
  0.0 377.1 jit_solution(16301794310421925368)
XLA Ops:
  6.5 0.0 all-gather.6.cloned.1.call-start
  6.5 0.7 all-gather.6.cloned.1.call-update
  7.3 0.0 all-gather.10.cloned.1.call-start
  7.3 0.7 all-gather.10.cloned.1.call-update
  8.0 0.0 all-gather.8.cloned.1.call-start
  8.1 0.7 all-gather.8.cloned.1.call-update
  8.7 0.0 all-gather.12.cloned.1.call-start
  8.8 0.5 all-gather.12.cloned.1.call-update
  9.3 0.0 reduce-scatter.3.cloned.1.call-start
  9.4 0.8 fusion.116
  10.1 0.8 fusion.113
  10.9 0.9 fusion.112
  11.8 0.9 fusion.111
  12.7 0.8 fusion.114
  13.5 16.3 %all-gather.6.cloned.1.call-done = bf16[320,2048]{1,0:T(8,128)(2,1)} async-done(((bf16[320,512]{1,0:T(8,128)(2,1)}), bf16[320,2048]{1,0:T(8,128)(2,1)}) %all-gather.6.cloned.1.call-update) | async-done | bytes 1310736 | tf_op jit(solution)/shard_map/all_gather | solution.py:27
  29.8 1.7 fusion
  31.5 73.3 %all-gather.10.cloned.1.call-done = bf16[2,2048,512]{2,1,0:T(8,128)(2,1)} async-done(((bf16[2,256,512]{2,1,0:T(8,128)(2,1)}), bf16[2,2048,512]{2,1,0:T(8,128)(2,1)}) %all-gather.10.cloned.1.call-update) | async-done | bytes 4194320 | tf_op jit(solution)/shard_map/all_gather | solution.py:23
  104.8 0.0 copy-start.1
  104.8 3.1 fusion.20
  107.9 0.0 copy-start.4
  107.9 70.4 %all-gather.8.cloned.1.call-done = bf16[2,2048,512]{2,1,0:T(8,128)(2,1)} async-done(((bf16[2,256,512]{2,1,0:T(8,128)(2,1)}), bf16[2,2048,512]{2,1,0:T(8,128)(2,1)}) %all-gather.8.cloned.1.call-update) | async-done | bytes 4194320 | tf_op jit(solution)/shard_map/all_gather | solution.py:22
  178.3 0.0 copy-done.1
  178.3 2.5 fusion.19
  180.8 2.5 collective-permute-start
  183.3 0.0 copy-done.4
  183.3 1.6 collective-permute-done
  184.9 0.1 maximum_convert_fusion
  185.0 3.2 fusion.107
  188.2 6.1 %all-reduce.1 = (f32[320,1]{0,1:T(1,128)S(1)}, f32[320,1]{0,1:T(1,128)S(1)}) all-reduce(f32[320,1]{0,1:T(1,128)S(1)} %broadcast_in_dim.20, f32[320,1]{0,1:T(1,128)S(1)} %broadcast_in_dim.21), channel_id=1, replica_groups=mesh['sp'=8,'tp'=4] {'tp'}, use_global_device_ids=true, to_apply=%region_2.0 | all-reduce | flops 640 | bytes 5120 | tf_op jit(solution)/shard_map/psum | solution.py:46
  194.3 59.2 %all-gather.12.cloned.1.call-done = bf16[2,512,2048]{2,1,0:T(8,128)(2,1)} async-done(((bf16[2,512,256]{2,1,0:T(8,128)(2,1)}), bf16[2,512,2048]{2,1,0:T(8,128)(2,1)}) %all-gather.12.cloned.1.call-update) | async-done | bytes 4194320 | tf_op jit(solution)/shard_map/all_gather | solution.py:25
  253.4 0.0 copy-start.5
  253.5 3.8 %convolution_convert_fusion.1 = bf16[320,2048]{1,0:T(8,128)(2,1)} fusion(bf16[2,512,2048]{2,1,0:T(8,128)(2,1)} %all-gather.12.cloned.1.call-done, f32[320,512]{1,0:T(8,128)S(1)} %get-tuple-element.18, f32[512]{0:T(512)S(1)} %bitcast.183, f32[512]{0:T(512)S(1)} %bitcast.182, f32[320]{0:T(512)S(1)} %get-tuple-element.12, f32[320]{0:T(512)S(1)} %get-tuple-element.11), kind=kOutput, calls=%fused_computation.5 | convolution fusion | flops 673218560 | bytes 4069888 | tf_op jit(solution)/shard_map/dot_general | solution.py:56
  257.2 0.0 reduce-scatter.3.cloned.1.call-update
  257.3 0.0 all-gather.14.cloned.1.call-start
  257.3 0.0 copy-done.5
  257.3 24.7 %reduce-scatter.3.cloned.1.call-done = bf16[320,512]{1,0:T(8,128)(2,1)} async-done(((bf16[320,2048]{1,0:T(8,128)(2,1)}), bf16[320,512]{1,0:T(8,128)(2,1)}) %reduce-scatter.3.cloned.1.call-update) | async-done | bytes 327696 | tf_op jit(solution)/shard_map/reduce_scatter | solution.py:57
  282.0 1.1 fusion.22
  283.2 5.8 %psum.44 = f32[320,1]{0,1:T(1,128)S(1)} all-reduce(f32[320,1]{0,1:T(1,128)S(1)} %broadcast_in_dim.22), channel_id=1, replica_groups=mesh['sp'=8,'tp'=4] {'tp'}, use_global_device_ids=true, to_apply=%region_7.8 | all-reduce | flops 320 | bytes 2560 | tf_op jit(solution)/shard_map/psum | solution.py:59
  288.9 0.0 copy-done.3
  289.0 1.9 fusion.25
  290.8 0.0 all-gather.14.cloned.1.call-update
  290.9 0.0 reduce-scatter.5.cloned.1.call-start
  290.9 18.9 %all-gather.14.cloned.1.call-done = bf16[320,2048]{1,0:T(8,128)(2,1)} async-done(((bf16[320,512]{1,0:T(8,128)(2,1)}), bf16[320,2048]{1,0:T(8,128)(2,1)}) %all-gather.14.cloned.1.call-update) | async-done | bytes 1310736 | tf_op jit(solution)/shard_map/all_gather | solution.py:27
  309.8 1.7 fusion.3
  311.5 0.0 copy-start.2
  311.5 0.0 copy-start.6
  311.5 3.1 fusion.21
  314.6 0.0 copy-done.2
  314.6 0.5 copy-done.6
  315.1 0.9 fusion.18
  316.0 3.4 collective-permute-start.1
  319.4 0.9 fusion.110
  320.3 0.7 collective-permute-done.1
  321.0 0.1 maximum_convert_fusion.1
  321.1 3.2 fusion.106
  324.3 6.0 %all-reduce = (f32[320,1]{0,1:T(1,128)S(1)}, f32[320,1]{0,1:T(1,128)S(1)}) all-reduce(f32[320,1]{0,1:T(1,128)S(1)} %broadcast_in_dim.23, f32[320,1]{0,1:T(1,128)S(1)} %broadcast_in_dim.24), channel_id=1, replica_groups=mesh['sp'=8,'tp'=4] {'tp'}, use_global_device_ids=true, to_apply=%region_10.11 | all-reduce | flops 640 | bytes 5120 | tf_op jit(solution)/shard_map/psum | solution.py:46
  330.3 0.0 copy-start
  330.3 3.7 convolution_convert_fusion
  334.0 0.0 reduce-scatter.5.cloned.1.call-update
  334.0 27.4 %reduce-scatter.5.cloned.1.call-done = bf16[320,512]{1,0:T(8,128)(2,1)} async-done(((bf16[320,2048]{1,0:T(8,128)(2,1)}), bf16[320,512]{1,0:T(8,128)(2,1)}) %reduce-scatter.5.cloned.1.call-update) | async-done | bytes 327696 | tf_op jit(solution)/shard_map/reduce_scatter | solution.py:57
  361.4 1.1 fusion.26
  362.5 5.8 %psum.47 = f32[320,1]{0,1:T(1,128)S(1)} all-reduce(f32[320,1]{0,1:T(1,128)S(1)} %broadcast_in_dim.25), channel_id=1, replica_groups=mesh['sp'=8,'tp'=4] {'tp'}, use_global_device_ids=true, to_apply=%region_15.16 | all-reduce | flops 320 | bytes 2560 | tf_op jit(solution)/shard_map/psum | solution.py:59
  368.3 0.0 copy-done
  368.3 1.9 fusion.29
  (17 shorter events, 0.2 us)
Async XLA Ops:
  6.5 23.3 %all-gather.6.cloned.1.call-start = ((), (), s32[]{:S(2)}) async-start(), calls=%async_computation.2 | async-start | bytes 1638400 | tf_op jit(solution)/shard_map/all_gather | solution.py:27
  7.3 97.5 %all-gather.10.cloned.1.call-start = ((), (), s32[]{:S(2)}) async-start(), calls=%async_computation.4 | async-start | bytes 4718592 | tf_op jit(solution)/shard_map/all_gather | solution.py:23
  8.0 170.3 %all-gather.8.cloned.1.call-start = ((), (), s32[]{:S(2)}) async-start(), calls=%async_computation.3 | async-start | bytes 4718592 | tf_op jit(solution)/shard_map/all_gather | solution.py:22
  8.7 244.7 %all-gather.12.cloned.1.call-start = ((), (), s32[]{:S(2)}) async-start(), calls=%async_computation.5 | async-start | bytes 4718592 | tf_op jit(solution)/shard_map/all_gather | solution.py:25
  9.3 272.7 %reduce-scatter.3.cloned.1.call-start = ((), (), s32[]{:S(2)}) async-start(), calls=%async_computation.6 | async-start | bytes 1638400 | tf_op jit(solution)/shard_map/reduce_scatter | solution.py:57
  104.8 73.5 %copy-start.1 = (bf16[320,2048]{1,0:T(8,128)(2,1)S(1)}, bf16[320,2048]{1,0:T(8,128)(2,1)}, u32[]{:S(2)}) copy-start(bf16[320,2048]{1,0:T(8,128)(2,1)} %all-gather.6.cloned.1.call-done) | copy-start | bytes 3932164
  107.9 75.4 %copy-start.4 = (f32[2,512]{1,0:T(2,128)S(1)}, f32[2,512]{1,0:T(2,128)}, u32[]{:S(2)}) copy-start(f32[2,512]{1,0:T(2,128)} %param.15) | copy-start | bytes 12292
  180.8 4.0 %collective-permute-start = (bf16[30,512]{1,0:T(8,128)(2,1)S(1)}, bf16[30,512]{1,0:T(8,128)(2,1)S(1)}, u32[]{:S(2)}, u32[]{:S(2)}) collective-permute-start(bf16[30,512]{1,0:T(8,128)(2,1)S(1)} %slice.562), channel_id=1, source_target_pairs={{0,4},{4,8},{8,12},{12,16},{16,20},{20,24},{24,28},{1,5},{5,9},{9,... | collective-permute-start | bytes 92168 | tf_op jit(solution)/shard_map/ppermute | solution.py:16
  253.4 3.9 %copy-start.5 = (f32[2,512]{1,0:T(2,128)S(1)}, f32[2,512]{1,0:T(2,128)}, u32[]{:S(2)}) copy-start(f32[2,512]{1,0:T(2,128)} %param.17) | copy-start | bytes 12292
  253.4 35.5 %copy-start.3 = (bf16[320,512]{1,0:T(8,128)(2,1)S(1)}, bf16[320,512]{1,0:T(8,128)(2,1)}, u32[]{:S(2)}) copy-start(bf16[320,512]{1,0:T(8,128)(2,1)} %param.9) | copy-start | bytes 983044
  257.3 52.5 %all-gather.14.cloned.1.call-start = ((), (), s32[]{:S(2)}) async-start(), calls=%async_computation.7 | async-start | bytes 1638400 | tf_op jit(solution)/shard_map/all_gather | solution.py:27
  290.9 70.5 %reduce-scatter.5.cloned.1.call-start = ((), (), s32[]{:S(2)}) async-start(), calls=%async_computation.8 | async-start | bytes 1638400 | tf_op jit(solution)/shard_map/reduce_scatter | solution.py:57
  311.5 3.1 copy-start.2
  311.5 3.6 copy-start.6
  316.0 5.0 %collective-permute-start.1 = (bf16[30,512]{1,0:T(8,128)(2,1)S(1)}, bf16[30,512]{1,0:T(8,128)(2,1)S(1)}, u32[]{:S(2)}, u32[]{:S(2)}) collective-permute-start(bf16[30,512]{1,0:T(8,128)(2,1)S(1)} %slice.597), channel_id=1, source_target_pairs={{0,4},{4,8},{8,12},{12,16},{16,20},{20,24},{24,28},{1,5},{5,9},{9,... | collective-permute-start | bytes 92168 | tf_op jit(solution)/shard_map/ppermute | solution.py:16
  330.3 38.1 %copy-start = (bf16[320,512]{1,0:T(8,128)(2,1)S(1)}, bf16[320,512]{1,0:T(8,128)(2,1)}, u32[]{:S(2)}) copy-start(bf16[320,512]{1,0:T(8,128)(2,1)} %fusion.25) | copy-start | bytes 983044
Sparse Core Ops, SparseCore 0:
  8.9 20.8 all-gather.5
  32.0 72.7 all-gather.9
  107.0 71.2 all-gather.7
  180.2 73.1 all-gather.11
  257.4 24.5 reduce-scatter.2
  291.0 18.7 all-gather.13
  334.1 27.2 reduce-scatter.4
where the time goes:
time: 378 us; the launch traced here: 377 us
  waiting for transfers between devices  295 us (78%)
  blocking collectives  23.5 us (6%)
  matrix products  17 us (4%)
  other arithmetic  16 us (4%)
  between operations  13.7 us (4%)
  starting transfers between devices  6.07 us (2%)
  local copies, waits for them, and re-layouts  5.61 us (1%)
    all_gather x1, waiting for transfers between devices, local(): lax.all_gather(w_gate, 'sp', axis=1, tiled=True)  73.3 us
    all_gather x1, waiting for transfers between devices, local(): lax.all_gather(w_value, 'sp', axis=1, tiled=True)  70.4 us
    all_gather x1, waiting for transfers between devices, local(): full_out = lax.all_gather(w_out, 'sp', axis=2, tiled=True)  59.2 us
    reduce_scatter x2, waiting for transfers between devices, local(): lax.psum_scatter(terms.astype(jnp.bfloat16), 'tp', scatter_dimension=1, t...  52.1 us
    all_gather x2, waiting for transfers between devices, local(): whole = lax.all_gather(stream, 'tp', axis=1, tiled=True)  35.2 us
    psum x2, blocking collectives, local(): lax.psum((jnp.sum(conv_out, -1, keepdims=True), jnp.sum(conv_out * conv_o...  12 us
    psum x2, blocking collectives, local(): lax.psum(jnp.sum(projected * projected, -1, keepdims=True), 'tp')  11.5 us
  transfers between devices with their start and end apart: 9, of which 9 were waited for; matrix products, arithmetic and copies ran while one was open for 4% of the time, Pallas kernels for 0%

commit v1 on v0

--- a/solution.py
+++ b/solution.py
@@ -8,6 +8,16 @@
 LAYERS = 2
 EPSILON = 1e-06
 LN_EPSILON = 1e-05
+
+
+def turned_line(x, axis, d):
+    size = lax.axis_size(axis)
+    current, pieces = (x, [x])
+    for _ in range(size - 1):
+        current = lax.ppermute(current, axis, [(i, (i + 1) % size) for i in range(size)])
+        pieces.insert(0, current)
+    merged = jnp.concatenate(pieces, axis=d)
+    return jnp.roll(merged, (lax.axis_index(axis) + 1) * x.shape[d], axis=d)
 
 
 def passed_along(block, axis, distance):
@@ -22,7 +32,7 @@
         lax.all_gather(w_value, "sp", axis=1, tiled=True),
         lax.all_gather(w_gate, "sp", axis=1, tiled=True),
     )
-    full_out = lax.all_gather(w_out, "sp", axis=2, tiled=True)
+    full_out = turned_line(w_out, "sp", 2)
     for layer in range(LAYERS):
         whole = lax.all_gather(stream, "tp", axis=1, tiled=True)
         whole_f = whole.astype(jnp.float32)

time: 378 us -> 363 us (0.960)
  waiting for transfers between devices: 295 us -> 258 us
  local copies, waits for them, and re-layouts: 5.61 us -> 24.7 us
    ppermute x0 -> x7, waiting for transfers between devices: none -> 137 us  [turned_line(): lax.ppermute(current, axis, [(i, (i + 1) % size) for i in range(size)])]
    all_gather x1, waiting for transfers between devices: 73.3 us -> 0.01 us  [local(): lax.all_gather(w_gate, 'sp', axis=1, tiled=True)]
    all_gather x1 -> x0, waiting for transfers between devices: 59.2 us -> none  [local(): full_out = lax.all_gather(w_out, 'sp', axis=2, tiled=True)]
    all_gather x1, waiting for transfers between devices: 70.4 us -> 44 us  [local(): lax.all_gather(w_value, 'sp', axis=1, tiled=True)]
    unnamed x14 -> x29, local copies, waits for them, and re-layouts: 0.5 us -> 18 us
    all_gather x2, waiting for transfers between devices: 35.2 us -> 18.9 us  [local(): whole = lax.all_gather(stream, 'tp', axis=1, tiled=True)]
  transfers between devices with their start and end apart: 9 -> 15, of which waited for: 9 -> 13; matrix products, arithmetic and copies ran while one was open for 4% -> 8% of each run, Pallas kernels for 0% -> 0%
where the time goes in v1:
time: 363 us; the launch traced here: 362 us
  waiting for transfers between devices  258 us (71%)
  local copies, waits for them, and re-layouts  24.7 us (7%)
  blocking collectives  23.3 us (6%)
  matrix products  17.1 us (5%)
  other arithmetic  16.1 us (4%)
  between operations  13.7 us (4%)
  starting transfers between devices  9.09 us (3%)
    ppermute x7, waiting for transfers between devices, turned_line(): lax.ppermute(current, axis, [(i, (i + 1) % size) for i in range(size)])  137 us
    reduce_scatter x2, waiting for transfers between devices, local(): lax.psum_scatter(terms.astype(jnp.bfloat16), 'tp', scatter_dimension=1, t...  55.4 us
    all_gather x1, waiting for transfers between devices, local(): lax.all_gather(w_value, 'sp', axis=1, tiled=True)  44 us
    all_gather x2, waiting for transfers between devices, local(): whole = lax.all_gather(stream, 'tp', axis=1, tiled=True)  18.9 us
    unnamed x29, local copies, waits for them, and re-layouts  18 us
    psum x2, blocking collectives, local(): lax.psum((jnp.sum(conv_out, -1, keepdims=True), jnp.sum(conv_out * conv_o...  11.7 us
    psum x2, blocking collectives, local(): lax.psum(jnp.sum(projected * projected, -1, keepdims=True), 'tp')  11.5 us
    dot_general x2, matrix products, local(): terms = jnp.dot(activated, out_mat, preferred_element_type=jnp.float32)  7.48 us
  transfers between devices with their start and end apart: 15, of which 13 were waited for; matrix products, arithmetic and copies ran while one was open for 8% of the time, Pallas kernels for 0%

profile of v1, /device:TPU:0, one launch (start us, length us, event | category | flops | bytes accessed | tf_op | source)
XLA Modules:
  0.0 362.2 jit_solution(6028497208586219525)
XLA Ops:
  6.5 0.7 all-gather.5.cloned.1.call-update
  7.3 0.7 all-gather.9.cloned.1.call-update
  8.1 0.7 all-gather.7.cloned.1.call-update
  8.8 3.0 collective-permute-start.1
  11.8 15.2 %collective-permute-done.1 = bf16[2,512,256]{2,1,0:T(8,128)(2,1)S(1)} collective-permute-done((bf16[2,512,256]{2,1,0:T(8,128)(2,1)}, bf16[2,512,256]{2,1,0:T(8,128)(2,1)S(1)}, u32[]{:S(2)}, u32[]{:S(2)}) %collective-permute-start.1) | collective-permute-done | bytes 524320 | tf_op jit(solution)/shard_map/ppermute | solution.py:17
  27.0 15.8 %collective-permute-done.2 = bf16[2,512,256]{2,1,0:T(8,128)(2,1)S(1)} collective-permute-done((bf16[2,512,256]{2,1,0:T(8,128)(2,1)S(1)}, bf16[2,512,256]{2,1,0:T(8,128)(2,1)S(1)}, u32[]{:S(2)}, u32[]{:S(2)}) %collective-permute-start.2) | collective-permute-done | bytes 524320 | tf_op jit(solution)/shard_map/ppermute | solution.py:17
  42.8 27.8 %collective-permute-done.3 = bf16[2,512,256]{2,1,0:T(8,128)(2,1)S(1)} collective-permute-done((bf16[2,512,256]{2,1,0:T(8,128)(2,1)S(1)}, bf16[2,512,256]{2,1,0:T(8,128)(2,1)S(1)}, u32[]{:S(2)}, u32[]{:S(2)}) %collective-permute-start.3) | collective-permute-done | bytes 524320 | tf_op jit(solution)/shard_map/ppermute | solution.py:17
  70.6 21.1 %collective-permute-done.4 = bf16[2,512,256]{2,1,0:T(8,128)(2,1)S(1)} collective-permute-done((bf16[2,512,256]{2,1,0:T(8,128)(2,1)S(1)}, bf16[2,512,256]{2,1,0:T(8,128)(2,1)S(1)}, u32[]{:S(2)}, u32[]{:S(2)}) %collective-permute-start.4) | collective-permute-done | bytes 524320 | tf_op jit(solution)/shard_map/ppermute | solution.py:17
  91.7 0.8 fusion.115
  92.5 0.9 fusion.113
  93.4 0.9 fusion.114
  94.3 24.3 %collective-permute-done.5 = bf16[2,512,256]{2,1,0:T(8,128)(2,1)S(1)} collective-permute-done((bf16[2,512,256]{2,1,0:T(8,128)(2,1)S(1)}, bf16[2,512,256]{2,1,0:T(8,128)(2,1)S(1)}, u32[]{:S(2)}, u32[]{:S(2)}) %collective-permute-start.5) | collective-permute-done | bytes 524320 | tf_op jit(solution)/shard_map/ppermute | solution.py:17
  118.7 0.8 fusion.119
  119.4 0.8 fusion.116
  120.3 22.7 %collective-permute-done.6 = bf16[2,512,256]{2,1,0:T(8,128)(2,1)} collective-permute-done((bf16[2,512,256]{2,1,0:T(8,128)(2,1)S(1)}, bf16[2,512,256]{2,1,0:T(8,128)(2,1)}, u32[]{:S(2)}, u32[]{:S(2)}) %collective-permute-start.6) | collective-permute-done | bytes 524320 | tf_op jit(solution)/shard_map/ppermute | solution.py:17
  142.9 0.8 fusion.118
  143.7 1.7 fusion
  145.5 9.7 %collective-permute-done.7 = bf16[2,512,256]{2,1,0:T(8,128)(2,1)} collective-permute-done((bf16[2,512,256]{2,1,0:T(8,128)(2,1)}, bf16[2,512,256]{2,1,0:T(8,128)(2,1)}, u32[]{:S(2)}, u32[]{:S(2)}) %collective-permute-start.7) | collective-permute-done | bytes 524320 | tf_op jit(solution)/shard_map/ppermute | solution.py:17
  155.1 2.0 constant_dynamic-update-slice_fusion.15
  157.1 1.9 constant_dynamic-update-slice_fusion.14
  159.0 0.9 constant_dynamic-update-slice_fusion.13
  159.9 0.9 constant_dynamic-update-slice_fusion.12
  160.8 0.9 constant_dynamic-update-slice_fusion.11
  161.6 0.9 constant_dynamic-update-slice_fusion.10
  162.5 0.9 constant_dynamic-update-slice_fusion.9
  163.4 0.9 constant_dynamic-update-slice_fusion.8
  164.3 2.0 constant_dynamic-update-slice_fusion.7
  166.2 1.9 constant_dynamic-update-slice_fusion.6
  168.1 0.9 constant_dynamic-update-slice_fusion.5
  169.0 0.9 constant_dynamic-update-slice_fusion.4
  169.9 0.9 constant_dynamic-update-slice_fusion.3
  170.8 0.9 constant_dynamic-update-slice_fusion.2
  171.7 0.9 constant_dynamic-update-slice_fusion.1
  172.6 3.1 fusion.20
  175.7 44.0 %all-gather.7.cloned.1.call-done = bf16[2,2048,512]{2,1,0:T(8,128)(2,1)} async-done(((bf16[2,256,512]{2,1,0:T(8,128)(2,1)}), bf16[2,2048,512]{2,1,0:T(8,128)(2,1)}) %all-gather.7.cloned.1.call-update) | async-done | bytes 4194320 | tf_op jit(solution)/shard_map/all_gather | solution.py:32
  219.7 2.5 fusion.19
  222.2 2.4 collective-permute-start
  224.7 0.9 constant_dynamic-update-slice_fusion
  225.5 0.7 collective-permute-done
  226.2 0.1 maximum_convert_fusion
  226.3 3.2 fusion.109
  229.5 5.7 %all-reduce.1 = (f32[320,1]{0,1:T(1,128)S(1)}, f32[320,1]{0,1:T(1,128)S(1)}) all-reduce(f32[320,1]{0,1:T(1,128)S(1)} %broadcast_in_dim.20, f32[320,1]{0,1:T(1,128)S(1)} %broadcast_in_dim.21), channel_id=1, replica_groups=mesh['sp'=8,'tp'=4] {'tp'}, use_global_device_ids=true, to_apply=%region_2.3 | all-reduce | flops 640 | bytes 5120 | tf_op jit(solution)/shard_map/psum | solution.py:56
  235.2 3.7 %convolution_convert_fusion.1 = bf16[320,2048]{1,0:T(8,128)(2,1)} fusion(bf16[2,512,4096]{2,1,0:T(8,128)(2,1)} %constant_dynamic-update-slice_fusion, s32[]{:T(128)S(6)} %select_n.14, f32[320,512]{1,0:T(8,128)S(1)} %get-tuple-element.18, f32[512]{0:T(512)S(1)} %bitcast.182, f32[512]{0:T(512)S(1)} %bitcast.183, f32[320]{0:T(512)S(1)} %get-tuple-element.12, ...), kind=kOutput, calls=%fused_computation.5 | convolution fusion | flops 673218560 | bytes 4069892 | tf_op jit(solution)/shard_map/dot_general | solution.py:66
  239.0 0.0 all-gather.11.cloned.1.call-start
  239.1 27.9 %reduce-scatter.3.cloned.1.call-done = bf16[320,512]{1,0:T(8,128)(2,1)} async-done(((bf16[320,2048]{1,0:T(8,128)(2,1)}), bf16[320,512]{1,0:T(8,128)(2,1)}) %reduce-scatter.3.cloned.1.call-update) | async-done | bytes 327696 | tf_op jit(solution)/shard_map/reduce_scatter | solution.py:67
  267.0 1.1 fusion.22
  268.1 5.8 %psum.44 = f32[320,1]{0,1:T(1,128)S(1)} all-reduce(f32[320,1]{0,1:T(1,128)S(1)} %broadcast_in_dim.22), channel_id=1, replica_groups=mesh['sp'=8,'tp'=4] {'tp'}, use_global_device_ids=true, to_apply=%region_7.8 | all-reduce | flops 320 | bytes 2560 | tf_op jit(solution)/shard_map/psum | solution.py:69
  273.9 1.9 fusion.25
  275.9 18.9 %all-gather.11.cloned.1.call-done = bf16[320,2048]{1,0:T(8,128)(2,1)} async-done(((bf16[320,512]{1,0:T(8,128)(2,1)}), bf16[320,2048]{1,0:T(8,128)(2,1)}) %all-gather.11.cloned.1.call-update) | async-done | bytes 1310736 | tf_op jit(solution)/shard_map/all_gather | solution.py:37
  294.8 1.7 fusion.3
  296.5 3.1 fusion.21
  299.6 0.5 copy-done.6
  300.1 0.9 fusion.18
  301.0 3.4 collective-permute-start.8
  304.4 0.9 fusion.112
  305.3 0.7 collective-permute-done.8
  306.0 0.1 maximum_convert_fusion.1
  306.1 3.2 fusion.108
  309.3 6.1 %all-reduce = (f32[320,1]{0,1:T(1,128)S(1)}, f32[320,1]{0,1:T(1,128)S(1)}) all-reduce(f32[320,1]{0,1:T(1,128)S(1)} %broadcast_in_dim.23, f32[320,1]{0,1:T(1,128)S(1)} %broadcast_in_dim.24), channel_id=1, replica_groups=mesh['sp'=8,'tp'=4] {'tp'}, use_global_device_ids=true, to_apply=%region_10.11 | all-reduce | flops 640 | bytes 5120 | tf_op jit(solution)/shard_map/psum | solution.py:56
  315.4 3.8 %convolution_convert_fusion = bf16[320,2048]{1,0:T(8,128)(2,1)} fusion(bf16[2,512,4096]{2,1,0:T(8,128)(2,1)} %constant_dynamic-update-slice_fusion, s32[]{:T(128)S(6)} %add.363, s32[]{:T(128)S(6)} %select_n.14, f32[320,512]{1,0:T(8,128)S(1)} %get-tuple-element.17, f32[512]{0:T(512)S(1)} %bitcast.180, f32[512]{0:T(512)S(1)} %bitcast.181, ...), kind=kOutput, calls=%fused_computation.4 | convolution fusion | flops 673218560 | bytes 4069896 | tf_op jit(solution)/shard_map/dot_general | solution.py:66
  319.2 27.4 %reduce-scatter.5.cloned.1.call-done = bf16[320,512]{1,0:T(8,128)(2,1)} async-done(((bf16[320,2048]{1,0:T(8,128)(2,1)}), bf16[320,512]{1,0:T(8,128)(2,1)}) %reduce-scatter.5.cloned.1.call-update) | async-done | bytes 327696 | tf_op jit(solution)/shard_map/reduce_scatter | solution.py:67
  346.6 1.1 fusion.26
  347.7 5.8 %psum.47 = f32[320,1]{0,1:T(1,128)S(1)} all-reduce(f32[320,1]{0,1:T(1,128)S(1)} %broadcast_in_dim.25), channel_id=1, replica_groups=mesh['sp'=8,'tp'=4] {'tp'}, use_global_device_ids=true, to_apply=%region_15.16 | all-reduce | flops 320 | bytes 2560 | tf_op jit(solution)/shard_map/psum | solution.py:69
  353.5 1.9 fusion.29
  (44 shorter events, 0.5 us)
Async XLA Ops:
  6.5 137.2 %all-gather.5.cloned.1.call-start = ((), (), s32[]{:S(2)}) async-start(), calls=%async_computation.2 | async-start | bytes 1638400 | tf_op jit(solution)/shard_map/all_gather | solution.py:37
  7.3 165.4 %all-gather.9.cloned.1.call-start = ((), (), s32[]{:S(2)}) async-start(), calls=%async_computation.4 | async-start | bytes 4718592 | tf_op jit(solution)/shard_map/all_gather | solution.py:33
  8.0 211.7 %all-gather.7.cloned.1.call-start = ((), (), s32[]{:S(2)}) async-start(), calls=%async_computation.3 | async-start | bytes 4718592 | tf_op jit(solution)/shard_map/all_gather | solution.py:32
  8.7 258.3 %reduce-scatter.3.cloned.1.call-start = ((), (), s32[]{:S(2)}) async-start(), calls=%async_computation.5 | async-start | bytes 1638400 | tf_op jit(solution)/shard_map/reduce_scatter | solution.py:67
  8.8 18.2 %collective-permute-start.1 = (bf16[2,512,256]{2,1,0:T(8,128)(2,1)}, bf16[2,512,256]{2,1,0:T(8,128)(2,1)S(1)}, u32[]{:S(2)}, u32[]{:S(2)}) collective-permute-start(bf16[2,512,256]{2,1,0:T(8,128)(2,1)} %param.16), channel_id=1, source_target_pairs={{0,4},{4,8},{8,12},{12,16},{16,20},{20,24},{24,28},{28,0},{1,5},{5... | collective-permute-start | bytes 1572872 | tf_op jit(solution)/shard_map/ppermute | solution.py:17
  27.0 15.8 %collective-permute-start.2 = (bf16[2,512,256]{2,1,0:T(8,128)(2,1)S(1)}, bf16[2,512,256]{2,1,0:T(8,128)(2,1)S(1)}, u32[]{:S(2)}, u32[]{:S(2)}) collective-permute-start(bf16[2,512,256]{2,1,0:T(8,128)(2,1)S(1)} %collective-permute-done.1), channel_id=1, source_target_pairs={{0,4},{4,8},{8,12},{12,16},{16,20},{20,24},{24,28},{28,0},{1,5},{5... | collective-permute-start | bytes 1572872 | tf_op jit(solution)/shard_map/ppermute | solution.py:17
  42.8 27.8 %collective-permute-start.3 = (bf16[2,512,256]{2,1,0:T(8,128)(2,1)S(1)}, bf16[2,512,256]{2,1,0:T(8,128)(2,1)S(1)}, u32[]{:S(2)}, u32[]{:S(2)}) collective-permute-start(bf16[2,512,256]{2,1,0:T(8,128)(2,1)S(1)} %collective-permute-done.2), channel_id=1, source_target_pairs={{0,4},{4,8},{8,12},{12,16},{16,20},{20,24},{24,28},{28,0},{1,5},{5... | collective-permute-start | bytes 1572872 | tf_op jit(solution)/shard_map/ppermute | solution.py:17
  70.6 21.1 %collective-permute-start.4 = (bf16[2,512,256]{2,1,0:T(8,128)(2,1)S(1)}, bf16[2,512,256]{2,1,0:T(8,128)(2,1)S(1)}, u32[]{:S(2)}, u32[]{:S(2)}) collective-permute-start(bf16[2,512,256]{2,1,0:T(8,128)(2,1)S(1)} %collective-permute-done.3), channel_id=1, source_target_pairs={{0,4},{4,8},{8,12},{12,16},{16,20},{20,24},{24,28},{28,0},{1,5},{5... | collective-permute-start | bytes 1572872 | tf_op jit(solution)/shard_map/ppermute | solution.py:17
  91.7 26.9 %collective-permute-start.5 = (bf16[2,512,256]{2,1,0:T(8,128)(2,1)S(1)}, bf16[2,512,256]{2,1,0:T(8,128)(2,1)S(1)}, u32[]{:S(2)}, u32[]{:S(2)}) collective-permute-start(bf16[2,512,256]{2,1,0:T(8,128)(2,1)S(1)} %collective-permute-done.4), channel_id=1, source_target_pairs={{0,4},{4,8},{8,12},{12,16},{16,20},{20,24},{24,28},{28,0},{1,5},{5... | collective-permute-start | bytes 1572872 | tf_op jit(solution)/shard_map/ppermute | solution.py:17
  118.7 24.3 %collective-permute-start.6 = (bf16[2,512,256]{2,1,0:T(8,128)(2,1)S(1)}, bf16[2,512,256]{2,1,0:T(8,128)(2,1)}, u32[]{:S(2)}, u32[]{:S(2)}) collective-permute-start(bf16[2,512,256]{2,1,0:T(8,128)(2,1)S(1)} %collective-permute-done.5), channel_id=1, source_target_pairs={{0,4},{4,8},{8,12},{12,16},{16,20},{20,24},{24,28},{28,0},{1,5},{5... | collective-permute-start | bytes 1572872 | tf_op jit(solution)/shard_map/ppermute | solution.py:17
  142.9 12.2 %collective-permute-start.7 = (bf16[2,512,256]{2,1,0:T(8,128)(2,1)}, bf16[2,512,256]{2,1,0:T(8,128)(2,1)}, u32[]{:S(2)}, u32[]{:S(2)}) collective-permute-start(bf16[2,512,256]{2,1,0:T(8,128)(2,1)} %collective-permute-done.6), channel_id=1, source_target_pairs={{0,4},{4,8},{8,12},{12,16},{16,20},{20,24},{24,28},{28,0},{1,5},{5... | collective-permute-start | bytes 1572872 | tf_op jit(solution)/shard_map/ppermute | solution.py:17
  143.7 19.7 %copy-start.1 = (bf16[2,512,256]{2,1,0:T(8,128)(2,1)S(1)}, bf16[2,512,256]{2,1,0:T(8,128)(2,1)}, u32[]{:S(2)}) copy-start(bf16[2,512,256]{2,1,0:T(8,128)(2,1)} %param.16) | copy-start | bytes 1572868
  172.6 47.1 %copy-start.2 = (bf16[320,2048]{1,0:T(8,128)(2,1)S(1)}, bf16[320,2048]{1,0:T(8,128)(2,1)}, u32[]{:S(2)}) copy-start(bf16[320,2048]{1,0:T(8,128)(2,1)} %all-gather.5.cloned.1.call-done) | copy-start | bytes 3932164
  222.2 4.0 %collective-permute-start = (bf16[30,512]{1,0:T(8,128)(2,1)S(1)}, bf16[30,512]{1,0:T(8,128)(2,1)S(1)}, u32[]{:S(2)}, u32[]{:S(2)}) collective-permute-start(bf16[30,512]{1,0:T(8,128)(2,1)S(1)} %slice.562), channel_id=1, source_target_pairs={{0,4},{4,8},{8,12},{12,16},{16,20},{20,24},{24,28},{1,5},{5,9},{9,... | collective-permute-start | bytes 92168 | tf_op jit(solution)/shard_map/ppermute | solution.py:26
  235.2 3.8 %copy-start.5 = (f32[2,512]{1,0:T(2,128)S(1)}, f32[2,512]{1,0:T(2,128)}, u32[]{:S(2)}) copy-start(f32[2,512]{1,0:T(2,128)} %param.17) | copy-start | bytes 12292
  235.2 38.7 %copy-start.4 = (bf16[320,512]{1,0:T(8,128)(2,1)S(1)}, bf16[320,512]{1,0:T(8,128)(2,1)}, u32[]{:S(2)}) copy-start(bf16[320,512]{1,0:T(8,128)(2,1)} %param.9) | copy-start | bytes 983044
  239.0 55.8 %all-gather.11.cloned.1.call-start = ((), (), s32[]{:S(2)}) async-start(), calls=%async_computation.6 | async-start | bytes 1638400 | tf_op jit(solution)/shard_map/all_gather | solution.py:37
  275.8 70.7 %reduce-scatter.5.cloned.1.call-start = ((), (), s32[]{:S(2)}) async-start(), calls=%async_computation.7 | async-start | bytes 1638400 | tf_op jit(solution)/shard_map/reduce_scatter | solution.py:67
  296.5 3.2 copy-start.3
  296.5 3.6 copy-start.6
  301.0 5.0 %collective-permute-start.8 = (bf16[30,512]{1,0:T(8,128)(2,1)S(1)}, bf16[30,512]{1,0:T(8,128)(2,1)S(1)}, u32[]{:S(2)}, u32[]{:S(2)}) collective-permute-start(bf16[30,512]{1,0:T(8,128)(2,1)S(1)} %slice.596), channel_id=1, source_target_pairs={{0,4},{4,8},{8,12},{12,16},{16,20},{20,24},{24,28},{1,5},{5,9},{9,... | collective-permute-start | bytes 92168 | tf_op jit(solution)/shard_map/ppermute | solution.py:26
  309.2 44.3 %copy-start = (bf16[320,512]{1,0:T(8,128)(2,1)S(1)}, bf16[320,512]{1,0:T(8,128)(2,1)}, u32[]{:S(2)}) copy-start(bf16[320,512]{1,0:T(8,128)(2,1)} %fusion.25) | copy-start | bytes 983044
Sparse Core Ops, SparseCore 0:
  8.9 20.8 all-gather.4
  32.0 101.0 all-gather.8
  135.3 84.3 all-gather.6
  239.1 27.8 reduce-scatter.2
  276.0 18.7 all-gather.10
  319.3 27.2 reduce-scatter.4
